TPU v7x, 32 devices: a whole 2x2x4 slice. The times are simulated.
32 devices in a mesh: sp: 8 (over z, x), tp: 4 (over y, core).
Axes of the slice: x: 2, y: 2, z: 4, core: 2. Of those that a mesh axis runs over, the one named last changes fastest.
Arguments:
- mixed: bfloat16 [1024, 2048], P('sp'), may hold values from -6 to 6
- cotangent: bfloat16 [1024, 2048], P('sp'), may hold values from -6 to 6
- routes: int32 [1024, 2], P('sp'), may hold values from 0 to 7, all different within a row; in each aligned block of 128 rows (0 to 127, 128 to 255, ...) at most 64 rows name the same one
- gates: float32 [1024, 2], P('sp'), may hold values from 0.1 to 1
- w_gate: bfloat16 [8, 2048, 1024], P('sp', None, 'tp'), may hold values from -0.125 to 0.125
- w_up: bfloat16 [8, 2048, 1024], P('sp', None, 'tp'), may hold values from -0.125 to 0.125
- w_down: bfloat16 [8, 1024, 2048], P('sp', 'tp'), may hold values from -0.1875 to 0.1875
- out_weight: bfloat16 [1024, 2048], P('tp'), may hold values from -0.1875 to 0.1875
- gate_pre: bfloat16 [1024, 1024], P('sp', 'tp'), may hold values from -8 to 8
- mixer_out: bfloat16 [1024, 1024], P('sp', 'tp'), may hold values from -6 to 6
- values: bfloat16 [1024, 1024], P('sp', 'tp'), may hold values from -6 to 6
- write_keys: bfloat16 [1024, 512], P('sp', 'tp'), may hold values from -1.25 to 1.25
- read_keys: bfloat16 [1024, 512], P('sp', 'tp'), may hold values from -1.25 to 1.25
- log_decay: float32 [16, 1024], P('tp', 'sp'), may hold values from -0.08 to 0
- entry_states: float32 [8, 16, 64, 128], P('sp', 'tp'), may hold values from -6 to 6
Outputs:
- d_w_gate: bfloat16 [8, 2048, 1024], P('sp', None, 'tp')
- d_w_up: bfloat16 [8, 2048, 1024], P('sp', None, 'tp')
- d_w_down: bfloat16 [8, 1024, 2048], P('sp', 'tp')
- d_out_weight: float32 [2048, 1024], P('sp', 'tp')
- d_input: bfloat16 [1024, 2048], P('sp', 'tp')
- d_values: bfloat16 [1024, 1024], P('sp', 'tp')
- d_write: float32 [1024, 512], P('sp', 'tp')
- d_read: float32 [1024, 512], P('sp', 'tp')
- d_gate: bfloat16 [1024, 1024], P('sp', 'tp')
Inputs may be any that keep to these rules, and one draw needn't show every extreme that they name: `routes`: each row names 2 different experts; in the 128 rows of one device no expert is named more than 64 times, and in some blocks one is named exactly 64 times.
All inputs are finite; a program needn't handle non-finite values.
Results may differ from a plain program's by a relative error of at most 0.0062.
Values may be sent and summed in bfloat16 or wider, within the bound.
A program may use at most 64 MiB of HBM per device.

v0:
```python
import jax
import jax.numpy as jnp
from jax import lax
from jax.sharding import PartitionSpec as P

D = 2048
HEAD_DIM = 64
BLOCK = 128
TOPK = 2
TOK_DEV = 128
precise = lax.Precision.HIGHEST


def prefix(part, axis, combine, identity):
    count = lax.axis_size(axis)
    place = lax.axis_index(axis)
    ahead = count - 1 - place
    gathered = jax.tree.map(lambda a: lax.all_gather(a, axis), part)
    state = jax.tree.map(lambda a, e: jnp.zeros_like(a) + jnp.asarray(e, a.dtype), part, identity)

    def one(lap, state):
        source = count - 1 - lap
        return combine(
            state, jax.tree.map(lambda a: lax.dynamic_index_in_dim(a, source, 0, False), gathered)
        )

    return lax.fori_loop(0, ahead, one, state)


def silu_grad(pre_act):
    logistic = jax.nn.sigmoid(pre_act)
    return logistic * (1.0 + pre_act * (1.0 - logistic))


def contract_rows(first_op, second_op):
    return lax.dot_general(
        first_op, second_op, (((0,), (0,)), ((), ())), preferred_element_type=jnp.float32
    )


def contract_cols(first_op, second_op):
    return lax.dot_general(
        first_op, second_op, (((1,), (1,)), ((), ())), preferred_element_type=jnp.float32
    )


def combine_state(earlier, later):
    return (later[0] * earlier[0], later[1] + later[0][:, None, None] * earlier[1])


def block_back(grad_state, inputs_x, grad_y, log_rate, write_rows, read_rows, start_state):
    block_len = log_rate.shape[0]
    running = jnp.cumsum(log_rate, axis=0)
    causal_mask = (jnp.arange(block_len)[:, None] >= jnp.arange(block_len)[None, :])[:, :, None]
    spread = running[:, None, :] - running[None, :, :]
    decay_mat = jnp.where(causal_mask, jnp.exp(jnp.where(causal_mask, spread, 0.0)), 0.0)
    intersection = jnp.dot(read_rows, write_rows.T, precision=precise)
    mixing = intersection[:, :, None] * decay_mat
    to_end = jnp.exp(running[-1][None, :] - running)
    from_start = jnp.exp(running)
    grad_x = jnp.einsum("lsj,ljp->sjp", mixing, grad_y, precision=precise) + to_end[
        :, :, None
    ] * jnp.einsum("sn,jpn->sjp", write_rows, grad_state, precision=precise)
    weighted = jnp.einsum("ljp,sjp->lsj", grad_y, inputs_x, precision=precise) * decay_mat
    grad_w = jnp.einsum("lsj,ln->sn", weighted, read_rows, precision=precise) + jnp.einsum(
        "sj,sjp,jpn->sn", to_end, inputs_x, grad_state, precision=precise
    )
    grad_r = jnp.einsum("lsj,sn->ln", weighted, write_rows, precision=precise) + jnp.einsum(
        "lj,ljp,jpn->ln", from_start, grad_y, start_state, precision=precise
    )
    earlier = jnp.exp(running[-1])[:, None, None] * grad_state + jnp.einsum(
        "lj,ljp,ln->jpn", from_start, grad_y, read_rows, precision=precise
    )
    return (earlier, grad_x, grad_w, grad_r)


def body(
    mixed,
    cotangent,
    routes,
    gates,
    w_gate,
    w_up,
    w_down,
    out_weight,
    gate_pre,
    mixer_out,
    values,
    write_keys,
    read_keys,
    log_decay,
    entry_states,
):
    sp_count = lax.axis_size("sp")
    tp_count = lax.axis_size("tp")
    capacity = 4 * TOK_DEV // sp_count
    assigned = TOK_DEV * TOPK
    picks = routes.reshape(assigned)
    onehot = (picks[:, None] == jnp.arange(sp_count, dtype=jnp.int32)[None, :]).astype(jnp.int32)
    earlier_same = jnp.cumsum(onehot, axis=0) - onehot
    slot_of = jnp.sum(earlier_same * onehot, axis=1)
    target = picks * capacity + slot_of
    anchor = (
        jnp.full((sp_count * capacity,), assigned, jnp.int32)
        .at[target]
        .set(jnp.arange(assigned, dtype=jnp.int32))
    )
    weight_g = w_gate[0]
    weight_u = w_up[0]
    weight_d = w_down[0]
    column_count = D // tp_count
    offset = lax.axis_index("tp") * column_count
    tok_slice = lax.dynamic_slice_in_dim(mixed, offset, column_count, 1)
    cot_slice = lax.dynamic_slice_in_dim(cotangent, offset, column_count, 1)
    columns = tok_slice.shape[1]
    scaled = (
        (gates[:, :, None] * cot_slice[:, None, :].astype(jnp.float32))
        .astype(jnp.bfloat16)
        .reshape(assigned, columns)
    )
    empty_row = jnp.zeros((1, columns), jnp.bfloat16)
    cot_buffer = jnp.concatenate([scaled, empty_row])[anchor].reshape(sp_count, capacity, columns)
    tok_buffer = jnp.concatenate([tok_slice, empty_row])[anchor // TOPK].reshape(
        sp_count, capacity, columns
    )
    tok_buffer, cot_buffer = (tok_buffer, cot_buffer)
    tok_part, cot_part = (
        lax.all_to_all(tok_buffer, "sp", split_axis=0, concat_axis=0, tiled=True),
        lax.all_to_all(cot_buffer, "sp", split_axis=0, concat_axis=0, tiled=True),
    )
    tok_rows, cot_rows = (
        lax.all_gather(tok_part, "tp", axis=2, tiled=True),
        lax.all_gather(cot_part, "tp", axis=2, tiled=True),
    )
    expert_tok_rows = tok_rows
    expert_cot_rows = cot_rows
    expert_tok_rows = expert_tok_rows.reshape(-1, D)
    expert_cot_rows = expert_cot_rows.reshape(-1, D)
    pre_gate = jnp.dot(expert_tok_rows, weight_g, preferred_element_type=jnp.float32)
    pre_up = jnp.dot(expert_tok_rows, weight_u, preferred_element_type=jnp.float32)
    active = jax.nn.silu(pre_gate)
    hidden = (active * pre_up).astype(jnp.bfloat16)
    grad_down = contract_rows(hidden, expert_cot_rows)
    grad_hidden = contract_cols(expert_cot_rows, weight_d)
    grad_gate = (grad_hidden * pre_up * silu_grad(pre_gate)).astype(jnp.bfloat16)
    grad_upval = (grad_hidden * active).astype(jnp.bfloat16)
    grad_wg = contract_rows(expert_tok_rows, grad_gate)
    grad_wu = contract_rows(expert_tok_rows, grad_upval)
    partial_value = contract_cols(grad_gate, weight_g) + contract_cols(grad_upval, weight_u)
    grad_wg, grad_wu, grad_down, partial_value = (grad_wg, grad_wu, grad_down, partial_value)
    row_total = partial_value.shape[0]
    pieces = partial_value.astype(jnp.bfloat16).reshape(row_total, tp_count, column_count)
    received = lax.all_to_all(pieces, "tp", split_axis=1, concat_axis=1, tiled=True)
    summed = (
        jnp.sum(received.astype(jnp.float32), axis=1)
        .astype(jnp.bfloat16)
        .reshape(sp_count, capacity, column_count)
    )
    returned = lax.all_to_all(summed, "sp", split_axis=0, concat_axis=0, tiled=True)
    columns = returned.shape[-1]
    picked = returned.reshape(sp_count * capacity, columns)[target].reshape(TOK_DEV, TOPK, columns)
    d_input = (cot_slice.astype(jnp.float32) + jnp.sum(picked.astype(jnp.float32), axis=1)).astype(
        jnp.bfloat16
    )
    whole = lax.all_gather(d_input, "tp", axis=1, tiled=True)
    back_proj = contract_cols(whole, out_weight)
    pre_act = gate_pre.astype(jnp.float32)
    gate_act = jax.nn.silu(pre_act)
    saved_out = mixer_out.astype(jnp.float32)
    d_gate = (back_proj * saved_out * silu_grad(pre_act)).astype(jnp.bfloat16)
    gated = (saved_out * gate_act).astype(jnp.bfloat16)
    d_out_weight = lax.psum_scatter(
        contract_rows(whole, gated), "sp", scatter_dimension=0, tiled=True
    )
    head_count = out_weight.shape[0] // HEAD_DIM
    grad_y = (back_proj * gate_act).reshape(TOK_DEV, head_count, HEAD_DIM)
    inputs_x = values.astype(jnp.float32).reshape(TOK_DEV, head_count, HEAD_DIM)
    write_rows = write_keys.astype(jnp.float32)
    read_rows = read_keys.astype(jnp.float32)
    log_rate = log_decay.T
    total_run = jnp.cumsum(log_rate, axis=0)
    shard_decay = jnp.exp(total_run[-1])
    shard_grad = jnp.einsum(
        "lj,ljp,ln->jpn", jnp.exp(total_run), grad_y, read_rows, precision=precise
    )
    identity = (jnp.ones_like(shard_decay), jnp.zeros_like(shard_grad))
    incoming = prefix((shard_decay, shard_grad), "sp", combine_state, identity)
    grad_state = incoming[1]
    pieces_x = []
    pieces_w = []
    pieces_r = []
    for block_id in reversed(range(TOK_DEV // BLOCK)):
        grad_state, grad_x, grad_w, grad_r = block_back(
            grad_state, inputs_x, grad_y, log_rate, write_rows, read_rows, entry_states[block_id]
        )
        pieces_x.insert(0, grad_x)
        pieces_w.insert(0, grad_w)
        pieces_r.insert(0, grad_r)
    d_values = pieces_x[0].reshape(TOK_DEV, head_count * HEAD_DIM).astype(jnp.bfloat16)
    d_write = pieces_w[0]
    d_read = pieces_r[0]
    return (
        grad_wg.astype(jnp.bfloat16)[None],
        grad_wu.astype(jnp.bfloat16)[None],
        grad_down.astype(jnp.bfloat16)[None],
        d_out_weight,
        d_input,
        d_values,
        d_write,
        d_read,
        d_gate,
    )


def solution(mesh):
    return jax.shard_map(
        body,
        mesh=mesh,
        in_specs=(
            P("sp", None),
            P("sp", None),
            P("sp", None),
            P("sp", None),
            P("sp", None, "tp"),
            P("sp", None, "tp"),
            P("sp", "tp", None),
            P("tp", None),
            P("sp", "tp"),
            P("sp", "tp"),
            P("sp", "tp"),
            P("sp", "tp"),
            P("sp", "tp"),
            P("tp", "sp"),
            P("sp", "tp", None, None),
        ),
        out_specs=(
            P("sp", None, "tp"),
            P("sp", None, "tp"),
            P("sp", "tp", None),
            P("sp", "tp"),
            P("sp", "tp"),
            P("sp", "tp"),
            P("sp", "tp"),
            P("sp", "tp"),
            P("sp", "tp"),
        ),
        check_vma=False,
    )
```

profile of v0, /device:TPU:0, one launch (start us, length us, event | category | flops | bytes accessed | tf_op | source)
XLA Modules:
  0.0 265.6 jit_solution(14270438159502153664)
XLA Ops:
  7.2 0.8 broadcast_multiply_fusion
  8.0 0.8 copy.51
  8.8 0.1 eq.29
  8.9 0.1 eq.25
  9.1 0.1 copy.50
  9.2 0.1 mul.130
  9.3 0.6 reduce-window.6
  9.9 0.2 slice_reduce_fusion
  10.3 1.4 scatter_custom_fusion
  11.7 1.0 dynamic-slice_convert_fusion
  12.8 2.0 gather_fusion
  14.8 21.7 %all_to_all.20 = bf16[8,64,512]{2,1,0:T(8,128)(2,1)} all-to-all(bf16[8,64,512]{2,1,0:T(8,128)(2,1)S(1)} %bitcast.115), channel_id=1, replica_groups=mesh['sp'=8,'tp'=4] {'sp'}, dimensions={0} | all-to-all | bytes 1048576 | tf_op jit(solution)/shard_map/all_to_all | solution.py:128
  36.5 0.2 mul.134
  36.7 0.4 mul.135
  37.2 0.1 mul.132
  37.5 2.0 gather_fusion.1
  39.5 17.6 %all_to_all.21 = bf16[8,64,512]{2,1,0:T(8,128)(2,1)} all-to-all(bf16[8,64,512]{2,1,0:T(8,128)(2,1)S(1)} %bitcast.116), channel_id=1, replica_groups=mesh['sp'=8,'tp'=4] {'sp'}, dimensions={0} | all-to-all | bytes 1048576 | tf_op jit(solution)/shard_map/all_to_all | solution.py:129
  57.1 1.1 all-gather.6.cloned.1.call-done
  58.3 2.5 fusion.10
  60.7 0.7 fusion.13
  61.5 20.9 %all-gather.8.cloned.1.call-done = bf16[8,64,2048]{2,1,0:T(8,128)(2,1)} async-done(((bf16[8,64,512]{2,1,0:T(8,128)(2,1)}), bf16[8,64,2048]{2,1,0:T(8,128)(2,1)}) %all-gather.8.cloned.1.call-update) | async-done | bytes 2097168 | tf_op jit(solution)/shard_map/all_gather | solution.py:133
  82.4 2.7 %multiply_convert_fusion.1 = (bf16[512,256]{1,0:T(8,128)(2,1)S(1)}, bf16[512,256]{1,0:T(8,128)(2,1)S(1)}) fusion(f32[512,256]{1,0:T(8,128)S(1)} %fusion.10, f32[512,256]{1,0:T(8,128)S(1)} %fusion.13, bf16[512,2048]{1,0:T(8,128)(2,1)} %bitcast.117, bf16[1,256,2048]{2,1,0:T(8,128)(2,1)} %param.23), kind=kOutput, calls=%fused_computation.36 | convolution fusion | flops 538574848 | bytes 4718592 | tf_op jit(solution)/shard_map/dot_general | solution.py:42
  85.1 0.7 fusion.8
  85.9 0.8 add_convert_fusion
  86.6 0.2 copy.68
  86.8 28.1 %all_to_all.22 = bf16[512,4,512]{2,0,1:T(8,128)(2,1)S(1)} all-to-all(bf16[512,4,512]{2,0,1:T(8,128)(2,1)S(1)} %bitcast.113), channel_id=1, replica_groups=mesh['sp'=8,'tp'=4] {'tp'}, dimensions={1} | all-to-all | bytes 4194304 | tf_op jit(solution)/shard_map/all_to_all | solution.py:153
  114.9 1.2 reduce_sum.47
  116.2 5.5 %all-to-all-start.3 = ((bf16[8,64,512]{2,1,0:T(8,128)(2,1)}), bf16[8,64,512]{2,1,0:T(8,128)(2,1)S(1)}, u32[]{:S(2)}, u32[]{:S(2)}) async-start(bf16[8,64,512]{2,1,0:T(8,128)(2,1)} %bitcast.119), calls=%async_computation.3 | async-start | bytes 1048576 | tf_op jit(solution)/shard_map/all_to_all | solution.py:159
  121.8 0.2 reduce_window_sum.29
  122.1 13.7 %all-to-all-done.3 = bf16[8,64,512]{2,1,0:T(8,128)(2,1)S(1)} async-done(((bf16[8,64,512]{2,1,0:T(8,128)(2,1)}), bf16[8,64,512]{2,1,0:T(8,128)(2,1)S(1)}, u32[]{:S(2)}, u32[]{:S(2)}) %all-to-all-start.3) | async-done | bytes 524320 | tf_op jit(solution)/shard_map/all_to_all | solution.py:159
  135.8 1.2 gather_fusion.2
  137.0 0.3 reshape.147
  137.3 0.6 reduce_sum.48
  138.0 0.9 add_convert_fusion.1
  138.9 6.5 %all_gather.21 = bf16[128,2048]{1,0:T(8,128)(2,1)S(1)} all-gather(bf16[128,512]{1,0:T(8,128)(2,1)S(1)} %add_convert_fusion.1), channel_id=1, replica_groups=mesh['sp'=8,'tp'=4] {'tp'}, dimensions={1}, use_global_device_ids=true | all-gather | bytes 655360 | tf_op jit(solution)/shard_map/all_gather | solution.py:165
  145.4 2.3 fusion.21
  147.9 0.9 fusion.36
  148.8 0.2 reduce-scatter.2.cloned.1.call-start
  149.0 1.8 fusion.39
  151.0 0.1 copy.63
  151.2 18.8 %all-gather.1 = f32[8,1,4]{2,1,0:T(1,128)S(1)} all-gather(f32[1,1,4]{2,1,0:T(1,128)S(1)} %get-tuple-element.153), channel_id=1, replica_groups=mesh['sp'=8,'tp'=4] {'sp'}, dimensions={0}, use_global_device_ids=true | all-gather | bytes 144 | tf_op jit(solution)/shard_map/all_gather | solution.py:18
  170.0 0.1 fusion.57
  170.2 3.5 %fusion = bf16[1,2048,256]{2,1,0:T(8,128)(2,1)} fusion(bf16[512,2048]{1,0:T(8,128)(2,1)} %bitcast.134, bf16[512,256]{1,0:T(8,128)(2,1)S(1)} %get-tuple-element.147), kind=kOutput, calls=%fused_computation.10 | convolution fusion | flops 537395200 | bytes 3407872 | tf_op jit(solution)/shard_map/dot_general | solution.py:36
  173.7 1.7 fusion.1
  175.4 0.4 copy-done.7
  175.9 1.8 fusion.2
  177.6 0.4 convolution_bitcast_fusion.3
  178.0 0.4 fusion.4
  178.4 0.8 convolution_add_fusion
  179.3 8.7 %all-gather.10.cloned.1.call-done = f32[32,64,128]{2,1,0:T(8,128)} async-done(((f32[4,64,128]{2,1,0:T(8,128)}), f32[32,64,128]{2,1,0:T(8,128)}) %all-gather.10.cloned.1.call-update) | async-done | bytes 1048592 | tf_op jit(solution)/shard_map/all_gather | solution.py:18
  188.0 7.2 %while.14 = (s32[]{:T(128)}, f32[4,64,128]{2,1,0:T(8,128)S(1)}, s32[]{:T(128)}, f32[8,4,64,128]{3,2,1,0:T(8,128)}, f32[8,4]{1,0:T(8,128)S(1)}, /*index=5*/s32[]{:T(128)}, s32[]{:T(128)}, s32[]{:T(128)}, s32[]{:T(128)}) while((s32[]{:T(128)}, f32[4,64,128]{2,1,0:T(8,128)S(1)}, s32[]{:T(128)}, f32[8,4,64,128]{3,2,1,0:T(8,128)}, ...), condition=%wide.region_9.10_spmd, body=%wide.region_8.9_spmd.sunk | while | flops 65542 | bytes 393419 | solution.py:27
  188.0 1.0 bitcast_add_fusion.2
  189.0 1.0 bitcast_add_fusion.2
  190.1 1.0 bitcast_add_fusion.2
  191.1 1.0 bitcast_add_fusion.2
  192.1 1.0 bitcast_add_fusion.2
  193.2 1.0 bitcast_add_fusion.2
  194.2 1.0 bitcast_add_fusion.2
  195.2 0.2 fusion.6
  195.5 0.5 fusion.7
  195.9 0.7 copy.64
  196.7 0.4 convolution_bitcast_fusion.4
  197.1 0.9 convolution_add_fusion.1
  198.0 61.1 %reduce-scatter.2.cloned.1.call-done = f32[256,256]{1,0:T(8,128)} async-done(((f32[2048,256]{1,0:T(8,128)}), f32[256,256]{1,0:T(8,128)}) %reduce-scatter.2.cloned.1.call-update) | async-done | bytes 262160 | tf_op jit(solution)/shard_map/reduce_scatter | solution.py:172
  (75 shorter events, 1.2 us)
Async XLA Ops:
  7.2 51.1 %copy-start = (bf16[1,2048,256]{2,1,0:T(8,128)(2,1)S(1)}, bf16[1,2048,256]{2,1,0:T(8,128)(2,1)}, u32[]{:S(2)}) copy-start(bf16[1,2048,256]{2,1,0:T(8,128)(2,1)} %param.21) | copy-start | bytes 3145732
  7.2 51.1 %all-gather.6.cloned.1.call-start = ((), (), s32[]{:S(2)}) async-start(), calls=%async_computation.5 | async-start | bytes 2621440 | tf_op jit(solution)/shard_map/all_gather | solution.py:132
  14.7 22.4 %copy-start.17 = (f32[128,2]{0,1:T(2,128)S(1)}, f32[128,2]{0,1:T(2,128)}, u32[]{:S(2)}) copy-start(f32[128,2]{0,1:T(2,128)} %param.20) | copy-start | bytes 3076
  36.5 45.9 %all-gather.8.cloned.1.call-start = ((), (), s32[]{:S(2)}) async-start(), calls=%async_computation.6 | async-start | bytes 2621440 | tf_op jit(solution)/shard_map/all_gather | solution.py:133
  57.1 3.6 %copy-start.2 = (bf16[1,2048,256]{2,1,0:T(8,128)(2,1)S(1)}, bf16[1,2048,256]{2,1,0:T(8,128)(2,1)}, u32[]{:S(2)}) copy-start(bf16[1,2048,256]{2,1,0:T(8,128)(2,1)} %param.22) | copy-start | bytes 3145732
  58.3 2.5 copy-start.18
  60.7 24.3 %copy-start.4 = (f32[512,256]{1,0:T(8,128)}, f32[512,256]{1,0:T(8,128)S(1)}, u32[]{:S(2)}) copy-start(f32[512,256]{1,0:T(8,128)S(1)} %fusion.10) | copy-start | bytes 1572868
  61.5 23.6 %copy-start.6 = (f32[512,256]{1,0:T(8,128)}, f32[512,256]{1,0:T(8,128)S(1)}, u32[]{:S(2)}) copy-start(f32[512,256]{1,0:T(8,128)S(1)} %fusion.13) | copy-start | bytes 1572868
  85.1 0.8 copy-start.10
  114.9 6.8 %copy-start.16 = (f32[4,128]{1,0:T(4,128)S(1)}, f32[4,128]{1,0:T(4,128)}, u32[]{:S(2)}) copy-start(f32[4,128]{1,0:T(4,128)} %param.30) | copy-start | bytes 6148
  116.2 19.7 %all-to-all-start.3 = ((bf16[8,64,512]{2,1,0:T(8,128)(2,1)}), bf16[8,64,512]{2,1,0:T(8,128)(2,1)S(1)}, u32[]{:S(2)}, u32[]{:S(2)}) async-start(bf16[8,64,512]{2,1,0:T(8,128)(2,1)} %bitcast.119), calls=%async_computation.3 | async-start | bytes 1048576 | tf_op jit(solution)/shard_map/all_to_all | solution.py:159
  121.7 66.3 %all-gather.10.cloned.1.call-start = ((), (), s32[]{:S(2)}) async-start(), calls=%async_computation.8 | async-start | bytes 1179648 | tf_op jit(solution)/shard_map/all_gather | solution.py:18
  135.8 9.6 %copy-start.13 = (bf16[128,256]{1,0:T(8,128)(2,1)S(1)}, bf16[128,256]{1,0:T(8,128)(2,1)}, u32[]{:S(2)}) copy-start(bf16[128,256]{1,0:T(8,128)(2,1)} %param.26) | copy-start | bytes 196612
  135.8 9.6 %copy-start.14 = (bf16[128,256]{1,0:T(8,128)(2,1)S(1)}, bf16[128,256]{1,0:T(8,128)(2,1)}, u32[]{:S(2)}) copy-start(bf16[128,256]{1,0:T(8,128)(2,1)} %param.25) | copy-start | bytes 196612
  137.3 10.5 %copy-start.9 = (bf16[128,128]{1,0:T(8,128)(2,1)S(1)}, bf16[128,128]{1,0:T(8,128)(2,1)}, u32[]{:S(2)}) copy-start(bf16[128,128]{1,0:T(8,128)(2,1)} %param.29) | copy-start | bytes 98308
  138.9 12.0 %copy-start.3 = (bf16[128,512]{1,0:T(8,128)(2,1)}, bf16[128,512]{1,0:T(8,128)(2,1)S(1)}, u32[]{:S(2)}) copy-start(bf16[128,512]{1,0:T(8,128)(2,1)S(1)} %add_convert_fusion.1) | copy-start | bytes 393220
  148.8 2.2 copy-start.15
  148.8 21.2 %copy-start.8 = (bf16[128,128]{1,0:T(8,128)(2,1)S(1)}, bf16[128,128]{1,0:T(8,128)(2,1)}, u32[]{:S(2)}) copy-start(bf16[128,128]{1,0:T(8,128)(2,1)} %param.28) | copy-start | bytes 98308
  148.8 110.2 %reduce-scatter.2.cloned.1.call-start = ((), (), s32[]{:S(2)}) async-start(), calls=%async_computation.7 | async-start | bytes 2359296 | tf_op jit(solution)/shard_map/reduce_scatter | solution.py:172
  170.2 3.5 %copy-start.11 = (bf16[512,256]{1,0:T(8,128)(2,1)S(1)}, bf16[512,256]{1,0:T(8,128)(2,1)}, u32[]{:S(2)}) copy-start(bf16[512,256]{1,0:T(8,128)(2,1)} %copy-done.10) | copy-start | bytes 786436
  170.2 3.5 %copy-start.19 = (bf16[8,64,2048]{2,1,0:T(8,128)(2,1)S(1)}, bf16[8,64,2048]{2,1,0:T(8,128)(2,1)}, u32[]{:S(2)}) copy-start(bf16[8,64,2048]{2,1,0:T(8,128)(2,1)} %all-gather.6.cloned.1.call-done) | copy-start | bytes 6291460
  173.7 1.8 copy-start.1
  173.7 1.8 copy-start.5
  173.7 2.2 copy-start.7
  175.9 1.8 copy-start.12
Sparse Core Ops, SparseCore 0:
  36.6 21.5 all-gather.5
  59.8 22.5 all-gather.7
  148.9 38.9 all-gather.9
  191.9 67.0 reduce-scatter.1
where the time goes:
time: 266 us
  waiting for transfers between devices  106 us (40%)
  blocking collectives  92.8 us (35%)
  matrix products  23.1 us (9%)
  between operations  14.2 us (5%)
  other arithmetic  12.6 us (5%)
  local copies, waits for them, and re-layouts  11.2 us (4%)
  starting transfers between devices  5.85 us (2%)
    reduce_scatter x1, waiting for transfers between devices, body(): lax.psum_scatter(contract_rows(whole, gated), 'sp', scatter_dimension=0,...  61.1 us
    all_to_all x1, blocking collectives, body(): lax.all_to_all(pieces, 'tp', split_axis=1, concat_axis=1, tiled=True)  28.1 us
    all_to_all x1, blocking collectives, body(): lax.all_to_all(tok_buffer, 'sp', split_axis=0, concat_axis=0, tiled=True)  21.7 us
    all_gather x1, waiting for transfers between devices, body(): lax.all_gather(cot_part, 'tp', axis=2, tiled=True)  20.9 us
    all_gather x1, blocking collectives, prefix(): gathered = jax.tree.map(lambda a: lax.all_gather(a, axis), part)  18.8 us
    all_to_all x1, blocking collectives, body(): lax.all_to_all(cot_buffer, 'sp', split_axis=0, concat_axis=0, tiled=True)  17.6 us
    all_to_all x1, waiting for transfers between devices, body(): lax.all_to_all(summed, 'sp', split_axis=0, concat_axis=0, tiled=True)  13.7 us
    dot_general x4, matrix products, contract_rows(): lax.dot_general(first_op, second_op, (((0,), (0,)), ((), ())), preferred_...  8.79 us
  transfers between devices with their start and end apart: 5, of which 5 were waited for; matrix products, arithmetic and copies ran while one was open for 10% of the time, Pallas kernels for 0%

commit v1 on v0

--- a/solution.py
+++ b/solution.py
@@ -1,3 +1,4 @@
+import functools
 import jax
 import jax.numpy as jnp
 from jax import lax
@@ -9,6 +10,16 @@
 TOPK = 2
 TOK_DEV = 128
 precise = lax.Precision.HIGHEST
+
+
+def match_task(vec, dim_i, dim_at):
+    f_now = jnp.stack(jnp.split(vec, lax.psum(1, axis_name="tp"), dim_i))
+    return jnp.concatenate(
+        lax.all_to_all(f_now, concat_axis=0, axis_name="tp", split_axis=0), dim_at
+    )
+
+
+choose_islands = functools.partial(match_task, dim_i=1, dim_at=1)
 
 
 def prefix(part, axis, combine, identity):
@@ -150,7 +161,7 @@
     grad_wg, grad_wu, grad_down, partial_value = (grad_wg, grad_wu, grad_down, partial_value)
     row_total = partial_value.shape[0]
     pieces = partial_value.astype(jnp.bfloat16).reshape(row_total, tp_count, column_count)
-    received = lax.all_to_all(pieces, "tp", split_axis=1, concat_axis=1, tiled=True)
+    received = choose_islands(pieces)
     summed = (
         jnp.sum(received.astype(jnp.float32), axis=1)
         .astype(jnp.bfloat16)

time: 266 us -> 275 us (1.034)
  local copies, waits for them, and re-layouts: 11.2 us -> 17.9 us
    reshape x1, local copies, waits for them, and re-layouts: 0.16 us -> 3.31 us  [body(): partial_value.astype(jnp.bfloat16)]
    split x0 -> x1, local copies, waits for them, and re-layouts: none -> 3.05 us  [match_task(): f_now = jnp.stack(jnp.split(vec, lax.psum(1, axis_name='tp'), dim_i))]
where the time goes in v1:
time: 275 us; the launch traced here: 274 us
  waiting for transfers between devices  106 us (39%)
  blocking collectives  92.8 us (34%)
  matrix products  24.4 us (9%)
  local copies, waits for them, and re-layouts  17.9 us (7%)
  between operations  14.2 us (5%)
  other arithmetic  12.9 us (5%)
  starting transfers between devices  5.85 us (2%)
    reduce_scatter x1, waiting for transfers between devices, body(): lax.psum_scatter(contract_rows(whole, gated), 'sp', scatter_dimension=0,...  61.1 us
    all_to_all x1, blocking collectives, match_task(): lax.all_to_all(f_now, concat_axis=0, axis_name='tp', split_axis=0)  28.1 us
    all_to_all x1, blocking collectives, body(): lax.all_to_all(tok_buffer, 'sp', split_axis=0, concat_axis=0, tiled=True)  21.7 us
    all_gather x1, waiting for transfers between devices, body(): lax.all_gather(cot_part, 'tp', axis=2, tiled=True)  20.9 us
    all_gather x1, blocking collectives, prefix(): gathered = jax.tree.map(lambda a: lax.all_gather(a, axis), part)  18.8 us
    all_to_all x1, blocking collectives, body(): lax.all_to_all(cot_buffer, 'sp', split_axis=0, concat_axis=0, tiled=True)  17.6 us
    all_to_all x1, waiting for transfers between devices, body(): lax.all_to_all(summed, 'sp', split_axis=0, concat_axis=0, tiled=True)  13.5 us
    all_gather x1, waiting for transfers between devices, prefix(): gathered = jax.tree.map(lambda a: lax.all_gather(a, axis), part)  8.92 us
  transfers between devices with their start and end apart: 5, of which 5 were waited for; matrix products, arithmetic and copies ran while one was open for 10% of the time, Pallas kernels for 0%

profile of v1, /device:TPU:0, one launch (start us, length us, event | category | flops | bytes accessed | tf_op | source)
XLA Modules:
  0.0 273.9 jit_solution(17687718839020685538)
XLA Ops:
  7.2 0.8 broadcast_multiply_fusion
  8.0 0.8 copy.58
  8.9 0.1 eq.25
  9.2 0.1 mul.130
  9.3 0.6 reduce-window.6
  9.9 0.2 slice_reduce_fusion
  10.3 1.4 scatter_custom_fusion
  11.7 1.0 dynamic-slice_convert_fusion
  12.8 2.0 gather_fusion
  14.8 21.7 %all_to_all.20 = bf16[8,64,512]{2,1,0:T(8,128)(2,1)} all-to-all(bf16[8,64,512]{2,1,0:T(8,128)(2,1)S(1)} %bitcast.121), channel_id=1, replica_groups=mesh['sp'=8,'tp'=4] {'sp'}, dimensions={0} | all-to-all | bytes 1048576 | tf_op jit(solution)/shard_map/all_to_all | solution.py:139
  36.5 0.2 mul.134
  36.7 0.4 mul.135
  37.2 0.1 mul.132
  37.5 2.0 gather_fusion.1
  39.5 17.6 %all_to_all.21 = bf16[8,64,512]{2,1,0:T(8,128)(2,1)} all-to-all(bf16[8,64,512]{2,1,0:T(8,128)(2,1)S(1)} %bitcast.122), channel_id=1, replica_groups=mesh['sp'=8,'tp'=4] {'sp'}, dimensions={0} | all-to-all | bytes 1048576 | tf_op jit(solution)/shard_map/all_to_all | solution.py:140
  57.1 1.1 all-gather.6.cloned.1.call-done
  58.3 2.5 fusion.10
  60.7 0.7 fusion.13
  61.5 20.9 %all-gather.8.cloned.1.call-done = bf16[8,64,2048]{2,1,0:T(8,128)(2,1)} async-done(((bf16[8,64,512]{2,1,0:T(8,128)(2,1)}), bf16[8,64,2048]{2,1,0:T(8,128)(2,1)}) %all-gather.8.cloned.1.call-update) | async-done | bytes 2097168 | tf_op jit(solution)/shard_map/all_gather | solution.py:144
  82.4 2.7 multiply_convert_fusion.1
  85.1 0.7 fusion.8
  85.9 2.1 add_convert_fusion
  88.0 3.3 %reshape.144 = bf16[512,4,512]{2,1,0:T(4,128)(2,1)S(1)} reshape(bf16[512,2048]{1,0:T(8,128)(2,1)} %add_convert_fusion) | data formatting | bytes 4194304 | tf_op jit(solution)/shard_map/reshape | solution.py:163
  91.3 3.1 %fusion.57 = (bf16[512,1,512]{2,1,0:T(2,128)(2,1)S(1)}, bf16[512,1,512]{2,1,0:T(2,128)(2,1)S(1)}, bf16[512,1,512]{2,1,0:T(2,128)(2,1)S(1)}, bf16[512,1,512]{2,1,0:T(2,128)(2,1)S(1)}) fusion(bf16[512,4,512]{2,1,0:T(4,128)(2,1)S(1)} %reshape.144), kind=kLoop, calls=%fused_computation.111 | loop fusion | bytes 4194304 | tf_op jit(solution)/shard_map/split | solution.py:16
  94.9 0.3 pad_maximum_fusion
  95.1 28.1 %all_to_all.22 = bf16[4,512,1,512]{3,1,2,0:T(8,128)(2,1)S(1)} all-to-all(bf16[4,512,1,512]{3,1,2,0:T(8,128)(2,1)S(1)} %pad_maximum_fusion), channel_id=1, replica_groups=mesh['sp'=8,'tp'=4] {'tp'}, dimensions={0} | all-to-all | bytes 4194304 | tf_op jit(solution)/shard_map/all_to_all | solution.py:18
  123.3 1.2 reduce_sum.47
  124.5 5.5 %all-to-all-start.3 = ((bf16[8,64,512]{2,1,0:T(8,128)(2,1)}), bf16[8,64,512]{2,1,0:T(8,128)(2,1)S(1)}, u32[]{:S(2)}, u32[]{:S(2)}) async-start(bf16[8,64,512]{2,1,0:T(8,128)(2,1)} %bitcast.125), calls=%async_computation.3 | async-start | bytes 1048576 | tf_op jit(solution)/shard_map/all_to_all | solution.py:170
  130.0 0.2 all-gather.10.cloned.1.call-start
  130.4 0.2 reduce_window_sum.29
  130.6 13.5 %all-to-all-done.3 = bf16[8,64,512]{2,1,0:T(8,128)(2,1)S(1)} async-done(((bf16[8,64,512]{2,1,0:T(8,128)(2,1)}), bf16[8,64,512]{2,1,0:T(8,128)(2,1)S(1)}, u32[]{:S(2)}, u32[]{:S(2)}) %all-to-all-start.3) | async-done | bytes 524320 | tf_op jit(solution)/shard_map/all_to_all | solution.py:170
  144.2 1.2 gather_fusion.2
  145.3 0.3 reshape.149
  145.7 0.6 reduce_sum.48
  146.3 0.9 add_convert_fusion.1
  147.3 6.5 %all_gather.21 = bf16[128,2048]{1,0:T(8,128)(2,1)S(1)} all-gather(bf16[128,512]{1,0:T(8,128)(2,1)S(1)} %add_convert_fusion.1), channel_id=1, replica_groups=mesh['sp'=8,'tp'=4] {'tp'}, dimensions={1}, use_global_device_ids=true | all-gather | bytes 655360 | tf_op jit(solution)/shard_map/all_gather | solution.py:176
  153.8 2.4 fusion.21
  156.2 0.9 fusion.36
  157.2 1.8 fusion.39
  159.2 0.1 copy.73
  159.3 18.8 %all-gather.1 = f32[8,1,4]{2,1,0:T(1,128)S(1)} all-gather(f32[1,1,4]{2,1,0:T(1,128)S(1)} %get-tuple-element.157), channel_id=1, replica_groups=mesh['sp'=8,'tp'=4] {'sp'}, dimensions={0}, use_global_device_ids=true | all-gather | bytes 144 | tf_op jit(solution)/shard_map/all_gather | solution.py:29
  178.2 0.2 fusion.58
  178.4 3.5 %fusion = bf16[1,2048,256]{2,1,0:T(8,128)(2,1)} fusion(bf16[512,2048]{1,0:T(8,128)(2,1)} %bitcast.144, bf16[512,256]{1,0:T(8,128)(2,1)S(1)} %get-tuple-element.151), kind=kOutput, calls=%fused_computation.10 | convolution fusion | flops 537395200 | bytes 3407872 | tf_op jit(solution)/shard_map/dot_general | solution.py:47
  181.9 1.8 fusion.1
  183.6 0.4 copy-done.7
  184.0 1.8 fusion.2
  185.7 0.4 convolution_bitcast_fusion.3
  186.1 0.4 fusion.4
  186.6 0.8 convolution_add_fusion
  187.4 8.9 %all-gather.10.cloned.1.call-done = f32[32,64,128]{2,1,0:T(8,128)} async-done(((f32[4,64,128]{2,1,0:T(8,128)}), f32[32,64,128]{2,1,0:T(8,128)}) %all-gather.10.cloned.1.call-update) | async-done | bytes 1048592 | tf_op jit(solution)/shard_map/all_gather | solution.py:29
  196.3 7.2 %while.14 = (s32[]{:T(128)}, f32[4,64,128]{2,1,0:T(8,128)S(1)}, s32[]{:T(128)}, f32[8,4,64,128]{3,2,1,0:T(8,128)}, f32[8,4]{1,0:T(8,128)S(1)}, /*index=5*/s32[]{:T(128)}, s32[]{:T(128)}, s32[]{:T(128)}, s32[]{:T(128)}) while((s32[]{:T(128)}, f32[4,64,128]{2,1,0:T(8,128)S(1)}, s32[]{:T(128)}, f32[8,4,64,128]{3,2,1,0:T(8,128)}, ...), condition=%wide.region_9.10_spmd, body=%wide.region_8.9_spmd.sunk | while | flops 65542 | bytes 393419 | solution.py:38
  196.3 1.0 bitcast_add_fusion.2
  197.4 1.0 bitcast_add_fusion.2
  198.4 1.0 bitcast_add_fusion.2
  199.5 1.0 bitcast_add_fusion.2
  200.5 1.0 bitcast_add_fusion.2
  201.5 1.0 bitcast_add_fusion.2
  202.6 1.0 bitcast_add_fusion.2
  203.6 0.2 fusion.6
  203.8 0.5 fusion.7
  204.3 0.7 copy.74
  205.0 0.4 convolution_bitcast_fusion.4
  205.4 0.9 convolution_add_fusion.1
  206.3 61.1 %reduce-scatter.2.cloned.1.call-done = f32[256,256]{1,0:T(8,128)} async-done(((f32[2048,256]{1,0:T(8,128)}), f32[256,256]{1,0:T(8,128)}) %reduce-scatter.2.cloned.1.call-update) | async-done | bytes 262160 | tf_op jit(solution)/shard_map/reduce_scatter | solution.py:183
  (81 shorter events, 2.0 us)
Async XLA Ops:
  7.2 51.1 %copy-start = (bf16[1,2048,256]{2,1,0:T(8,128)(2,1)S(1)}, bf16[1,2048,256]{2,1,0:T(8,128)(2,1)}, u32[]{:S(2)}) copy-start(bf16[1,2048,256]{2,1,0:T(8,128)(2,1)} %param.21) | copy-start | bytes 3145732
  7.2 51.1 %all-gather.6.cloned.1.call-start = ((), (), s32[]{:S(2)}) async-start(), calls=%async_computation.5 | async-start | bytes 2621440 | tf_op jit(solution)/shard_map/all_gather | solution.py:143
  14.7 22.4 %copy-start.17 = (f32[128,2]{0,1:T(2,128)S(1)}, f32[128,2]{0,1:T(2,128)}, u32[]{:S(2)}) copy-start(f32[128,2]{0,1:T(2,128)} %param.20) | copy-start | bytes 3076
  36.5 45.9 %all-gather.8.cloned.1.call-start = ((), (), s32[]{:S(2)}) async-start(), calls=%async_computation.6 | async-start | bytes 2621440 | tf_op jit(solution)/shard_map/all_gather | solution.py:144
  57.1 3.6 %copy-start.2 = (bf16[1,2048,256]{2,1,0:T(8,128)(2,1)S(1)}, bf16[1,2048,256]{2,1,0:T(8,128)(2,1)}, u32[]{:S(2)}) copy-start(bf16[1,2048,256]{2,1,0:T(8,128)(2,1)} %param.22) | copy-start | bytes 3145732
  58.3 2.5 copy-start.18
  60.7 24.3 %copy-start.4 = (f32[512,256]{1,0:T(8,128)}, f32[512,256]{1,0:T(8,128)S(1)}, u32[]{:S(2)}) copy-start(f32[512,256]{1,0:T(8,128)S(1)} %fusion.10) | copy-start | bytes 1572868
  61.5 23.6 %copy-start.6 = (f32[512,256]{1,0:T(8,128)}, f32[512,256]{1,0:T(8,128)S(1)}, u32[]{:S(2)}) copy-start(f32[512,256]{1,0:T(8,128)S(1)} %fusion.13) | copy-start | bytes 1572868
  85.1 0.8 copy-start.10
  123.3 7.0 %copy-start.16 = (f32[4,128]{1,0:T(4,128)S(1)}, f32[4,128]{1,0:T(4,128)}, u32[]{:S(2)}) copy-start(f32[4,128]{1,0:T(4,128)} %param.30) | copy-start | bytes 6148
  124.5 19.7 %all-to-all-start.3 = ((bf16[8,64,512]{2,1,0:T(8,128)(2,1)}), bf16[8,64,512]{2,1,0:T(8,128)(2,1)S(1)}, u32[]{:S(2)}, u32[]{:S(2)}) async-start(bf16[8,64,512]{2,1,0:T(8,128)(2,1)} %bitcast.125), calls=%async_computation.3 | async-start | bytes 1048576 | tf_op jit(solution)/shard_map/all_to_all | solution.py:170
  130.0 66.3 %all-gather.10.cloned.1.call-start = ((), (), s32[]{:S(2)}) async-start(), calls=%async_computation.8 | async-start | bytes 1179648 | tf_op jit(solution)/shard_map/all_gather | solution.py:29
  144.2 9.6 %copy-start.13 = (bf16[128,256]{1,0:T(8,128)(2,1)S(1)}, bf16[128,256]{1,0:T(8,128)(2,1)}, u32[]{:S(2)}) copy-start(bf16[128,256]{1,0:T(8,128)(2,1)} %param.26) | copy-start | bytes 196612
  144.2 9.6 %copy-start.14 = (bf16[128,256]{1,0:T(8,128)(2,1)S(1)}, bf16[128,256]{1,0:T(8,128)(2,1)}, u32[]{:S(2)}) copy-start(bf16[128,256]{1,0:T(8,128)(2,1)} %param.25) | copy-start | bytes 196612
  145.7 10.5 %copy-start.9 = (bf16[128,128]{1,0:T(8,128)(2,1)S(1)}, bf16[128,128]{1,0:T(8,128)(2,1)}, u32[]{:S(2)}) copy-start(bf16[128,128]{1,0:T(8,128)(2,1)} %param.29) | copy-start | bytes 98308
  147.3 11.8 %copy-start.3 = (bf16[128,512]{1,0:T(8,128)(2,1)}, bf16[128,512]{1,0:T(8,128)(2,1)S(1)}, u32[]{:S(2)}) copy-start(bf16[128,512]{1,0:T(8,128)(2,1)S(1)} %add_convert_fusion.1) | copy-start | bytes 393220
  157.1 2.1 copy-start.15
  157.1 21.1 %copy-start.8 = (bf16[128,128]{1,0:T(8,128)(2,1)S(1)}, bf16[128,128]{1,0:T(8,128)(2,1)}, u32[]{:S(2)}) copy-start(bf16[128,128]{1,0:T(8,128)(2,1)} %param.28) | copy-start | bytes 98308
  157.2 110.2 %reduce-scatter.2.cloned.1.call-start = ((), (), s32[]{:S(2)}) async-start(), calls=%async_computation.7 | async-start | bytes 2359296 | tf_op jit(solution)/shard_map/reduce_scatter | solution.py:183
  178.4 3.5 %copy-start.11 = (bf16[512,256]{1,0:T(8,128)(2,1)S(1)}, bf16[512,256]{1,0:T(8,128)(2,1)}, u32[]{:S(2)}) copy-start(bf16[512,256]{1,0:T(8,128)(2,1)} %copy-done.10) | copy-start | bytes 786436
  178.4 3.5 %copy-start.19 = (bf16[8,64,2048]{2,1,0:T(8,128)(2,1)S(1)}, bf16[8,64,2048]{2,1,0:T(8,128)(2,1)}, u32[]{:S(2)}) copy-start(bf16[8,64,2048]{2,1,0:T(8,128)(2,1)} %all-gather.6.cloned.1.call-done) | copy-start | bytes 6291460
  181.8 1.8 copy-start.1
  181.8 1.8 copy-start.5
  181.9 2.1 copy-start.7
  184.0 1.8 copy-start.12
Sparse Core Ops, SparseCore 0:
  36.6 21.5 all-gather.5
  59.8 22.5 all-gather.7
  157.3 38.9 all-gather.9
  200.3 67.0 reduce-scatter.1
